TPU v7x, 32 devices: a whole 2x2x4 slice. The times are simulated.
32 devices in a mesh: sp: 8 (over z, x), tp: 4 (over y, core).
Axes of the slice: x: 2, y: 2, z: 4, core: 2. Of those that a mesh axis runs over, the one named last changes fastest.
Arguments:
- latent: bfloat16 [4096, 2048], P(('sp', 'tp')), may hold values from -6 to 6
- context: bfloat16 [512, 2048], P('sp'), may hold values from -6 to 6
- conditioning: float32 [2048], P('sp'), may hold values from -6 to 6
- context_conditioning: float32 [2048], P('sp'), may hold values from -6 to 6
- shift_weight: bfloat16 [2048, 2048], P('sp', 'tp'), may hold values from -0.25 to 0.25
- scale_weight: bfloat16 [2048, 2048], P('sp', 'tp'), may hold values from -0.25 to 0.25
- gate_weight: bfloat16 [2048, 2048], P('sp', 'tp'), may hold values from -0.25 to 0.25
- norm_gain: float32 [2048], replicated, may hold values from 0.1 to 1.9
- query_weight: bfloat16 [2048, 2048], P(None, 'tp'), may hold values from -0.125 to 0.125
- key_weight: bfloat16 [2048, 1024], P(None, 'tp'), may hold values from -0.125 to 0.125
- value_weight: bfloat16 [2048, 1024], P(None, 'tp'), may hold values from -0.125 to 0.125
- query_gain: float32 [64], replicated, may hold values from 2 to 64, as said below
- key_gain: float32 [64], replicated, may hold values from 0.1 to 1.9
- context_lift: float32 [32], P('tp'), may hold values from 1.5 to 3
- output_weight: bfloat16 [2048, 2048], P('tp'), may hold values from -0.125 to 0.125
Outputs:
- mixed: bfloat16 [4096, 2048], P(('sp', 'tp'))
Inputs may be any that keep to these rules, and one draw needn't show every extreme that they name: `query_gain`: one gain for each channel of a head.
All inputs are finite; a program needn't handle non-finite values.
Results may differ from a plain program's by a relative error of at most 0.018.
The roundings to bfloat16 on the way count: a program that leaves them out, or rounds other values in their place, can miss the bound.
Values may be sent and summed in bfloat16 or wider, within the bound.
A program may use at most 128 MiB of HBM per device.

v0:
```python
import functools

import jax
import jax.numpy as jnp
from jax import lax
from jax.experimental import pallas as pl
from jax.experimental.pallas import tpu as pltpu
from jax.sharding import PartitionSpec as P

HEAD = 64
GRID = 64
EPSILON = 1e-06
ROTARY_BASE = 10000.0
F32 = jnp.float32
BF16 = jnp.bfloat16
VMEM = pltpu.VMEM


def dot(a, b):
    return jnp.dot(a, b, preferred_element_type=F32)


def remote(src, dst, send, recv, sp, tp):
    return pltpu.make_async_remote_copy(
        src_ref=src,
        dst_ref=dst,
        send_sem=send,
        recv_sem=recv,
        device_id=(sp, tp),
        device_id_type=pl.DeviceIdType.MESH,
    )


def project_kernel(
    n_sp, n_tp, q_heads, k_heads,
    latent_h, context_h, cond, ctx_cond, shift_h, scale_h, gate_h, gain,
    wq_h, wk_h, wv_h, q_gain, k_gain, cos_t, sin_t,
    qz, kv, call, gate_out,
    latent, context, shift_w, scale_w, gate_w, wq, wk, wv,
    lat, ckv, part, total, recv1, recv2, mods,
    s1, r1, s2, r2, sy, ry, sp_own, sp_fwd, rp, sc, rc, loads,
):
    fetch = [
        pltpu.make_async_copy(src, dst, loads.at[i])
        for i, (src, dst) in enumerate(
            (
                (latent_h, latent), (shift_h, shift_w), (scale_h, scale_w), (gate_h, gate_w),
                (context_h, context), (wk_h, wk), (wv_h, wv), (wq_h, wq),
            )
        )
    ]
    for copy in fetch:
        copy.start()
    me = lax.axis_index("sp")
    t = lax.axis_index("tp")
    n_y = n_tp // 2
    y, c = t // 2, t % 2
    partner = y * 2 + 1 - c
    barrier = pltpu.get_barrier_semaphore()

    def greet_sp(j, _):
        pl.semaphore_signal(barrier, inc=1, device_id=(lax.rem(me + j, n_sp), t), device_id_type=pl.DeviceIdType.MESH)
        return 0

    def greet_tp(j, _):
        pl.semaphore_signal(barrier, inc=1, device_id=(me, lax.rem(t + j, n_tp)), device_id_type=pl.DeviceIdType.MESH)
        return 0

    lax.fori_loop(1, n_sp, greet_sp, 0)
    lax.fori_loop(1, n_tp, greet_tp, 0)
    pl.semaphore_wait(barrier, n_sp + n_tp - 2)
    fetch[0].wait()

    def y_copy(k):
        other = lax.rem(y + k, n_y)
        return remote(latent, lat.at[t], sy.at[k], ry.at[t], me, other * 2 + c)

    def y_start(k, _):
        y_copy(k).start()
        return 0

    lax.fori_loop(1, n_y, y_start, 0)
    own_partner = remote(latent, lat.at[t], sp_own, rp.at[t], me, partner)
    own_partner.start()

    rows = lax.broadcasted_iota(jnp.int32, (8, cond.shape[1]), 0)
    a = jnp.broadcast_to(cond[...] / (1.0 + jnp.exp(-cond[...])), rows.shape)
    b = jnp.broadcast_to(ctx_cond[...] / (1.0 + jnp.exp(-ctx_cond[...])), rows.shape)
    first = jnp.where(rows == 0, a, jnp.where(rows == 1, b, 0.0)).astype(BF16)
    second = jnp.where(rows == 2, a, jnp.where(rows == 3, b, 0.0)).astype(BF16)
    third = jnp.where(rows == 4, a, 0.0).astype(BF16)
    for copy in fetch[1:4]:
        copy.wait()
    mine = dot(first, shift_w[...]) + dot(second, scale_w[...]) + dot(third, gate_w[...])
    part[...] = mine
    recv1[me] = mine

    def mod_copy(j):
        return remote(part, recv1.at[me], s1.at[j], r1.at[me], lax.rem(me + j, n_sp), t)

    def mod_start(j, _):
        mod_copy(j).start()
        return 0

    def mod_wait(j, _):
        src = lax.rem(me + j, n_sp)
        pltpu.make_async_copy(recv1.at[src], recv1.at[src], r1.at[src]).wait()
        return 0

    lax.fori_loop(1, n_sp, mod_start, 0)
    lax.fori_loop(1, n_sp, mod_wait, 0)
    summed = lax.fori_loop(1, n_sp, lambda j, s: s + recv1[j], recv1[0])
    total[...] = summed
    recv2[t] = summed

    def tot_copy(j):
        return remote(total, recv2.at[t], s2.at[j], r2.at[t], me, lax.rem(t + j, n_tp))

    def tot_start(j, _):
        tot_copy(j).start()
        return 0

    def tot_wait(j, _):
        src = lax.rem(t + j, n_tp)
        pltpu.make_async_copy(recv2.at[src], recv2.at[src], r2.at[src]).wait()
        return 0

    lax.fori_loop(1, n_tp, tot_start, 0)
    lax.fori_loop(1, n_tp, tot_wait, 0)
    width = total.shape[1]
    for j in range(n_tp):
        mods[:, j * width : (j + 1) * width] = recv2[j]
    gate_out[...] = mods[4:5, :]

    def hidden_of(x, shift_row, scale_row):
        x = x.astype(F32)
        inv = lax.rsqrt(jnp.mean(x * x, axis=-1, keepdims=True) + EPSILON)
        return (
            x * inv * gain[...] * (1.0 + mods[scale_row : scale_row + 1, :])
            + mods[shift_row : shift_row + 1, :]
        ).astype(BF16)

    def head_norm(v, gains):
        w = v.shape[1]
        heads_r = lax.broadcasted_iota(jnp.int32, (w, w), 0) // HEAD
        heads_c = lax.broadcasted_iota(jnp.int32, (w, w), 1) // HEAD
        ones = jnp.where(heads_r == heads_c, 1.0, 0.0).astype(BF16)
        sq = v * v
        hi = sq.astype(BF16)
        rest = sq - hi.astype(F32)
        mid = rest.astype(BF16)
        low = (rest - mid.astype(F32)).astype(BF16)
        mean = (dot(hi, ones) + (dot(mid, ones) + dot(low, ones))) * (1.0 / HEAD)
        return v * lax.rsqrt(mean + EPSILON) * jnp.concatenate([gains] * (w // 128), axis=1)

    def turn(v, cos_v, sin_v):
        w = v.shape[1]
        even = lax.broadcasted_iota(jnp.int32, v.shape, 1) % 2 == 0
        swapped = jnp.where(even, pltpu.roll(v, w - 1, 1), pltpu.roll(v, 1, 1))
        many = w // 128
        return v * jnp.concatenate([cos_v] * many, axis=1) + swapped * jnp.concatenate([sin_v] * many, axis=1)

    k_width = wk.shape[1]
    group = q_heads // k_heads

    def process(tiles, x):
        h = hidden_of(x, 0, 2)
        cos_v = jnp.concatenate([cos_t[tile] for tile in tiles], axis=0)
        sin_v = jnp.concatenate([sin_t[tile] for tile in tiles], axis=0)
        q = turn(head_norm(dot(h, wq[...]), q_gain[...]), cos_v, sin_v)
        per = q.shape[0] // len(tiles)
        low_half = lax.broadcasted_iota(jnp.int32, (q.shape[0], 128), 1) < HEAD
        for head in range(q_heads):
            piece = q[:, (head // 2) * 128 : (head // 2) * 128 + 128].astype(BF16).astype(F32) * HEAD ** (-0.5)
            side = (head // group) % 2
            if head % 2 != side:
                piece = pltpu.roll(piece, HEAD, 1)
            keep = low_half if side == 0 else jnp.logical_not(low_half)
            piece = jnp.where(keep, piece, 0.0)
            for i, tile in enumerate(tiles):
                qz[head, tile] = piece[i * per : (i + 1) * per].astype(BF16)
        k = turn(head_norm(dot(h, wk[...]), k_gain[...]), cos_v, sin_v)
        v = dot(h, wv[...])
        for i, tile in enumerate(tiles):
            kv[tile, :, :k_width] = k[i * per : (i + 1) * per].astype(BF16)
            kv[tile, :, k_width:] = v[i * per : (i + 1) * per].astype(BF16)

    for copy in fetch[4:]:
        copy.wait()
    hc = hidden_of(context[...], 1, 3)
    ckv[:, :k_width] = head_norm(dot(hc, wk[...]), k_gain[...]).astype(BF16)
    ckv[:, k_width:] = dot(hc, wv[...]).astype(BF16)

    def c_copy(j):
        return remote(ckv, call.at[me], sc.at[j], rc.at[me], lax.rem(me + j, n_sp), t)

    def c_start(j, _):
        c_copy(j).start()
        return 0

    lax.fori_loop(1, n_sp, c_start, 0)
    call[me] = ckv[...]

    def pair_of(first, second):
        return jnp.concatenate([first.astype(F32), second.astype(F32)], axis=0)

    pltpu.make_async_copy(lat.at[partner], lat.at[partner], rp.at[partner]).wait()
    process((t, partner), pair_of(latent[...], lat[partner]))

    def others(k, _):
        other = lax.rem(y + n_y - k, n_y)
        near, far = other * 2 + c, other * 2 + 1 - c
        pltpu.make_async_copy(lat.at[near], lat.at[near], ry.at[near]).wait()
        remote(lat.at[near], lat.at[near], sp_fwd.at[k], rp.at[near], me, partner).start()
        pltpu.make_async_copy(lat.at[far], lat.at[far], rp.at[far]).wait()
        process((near, far), pair_of(lat[near], lat[far]))
        return 0

    lax.fori_loop(1, n_y, others, 0)

    def c_wait(j, _):
        src = lax.rem(me + j, n_sp)
        pltpu.make_async_copy(call.at[src], call.at[src], rc.at[src]).wait()
        c_copy(j).wait_send()
        return 0

    lax.fori_loop(1, n_sp, c_wait, 0)

    def drain_y(k, _):
        y_copy(k).wait_send()
        other = lax.rem(y + n_y - k, n_y)
        near = other * 2 + c
        remote(lat.at[near], lat.at[near], sp_fwd.at[k], rp.at[near], me, partner).wait_send()
        return 0

    lax.fori_loop(1, n_y, drain_y, 0)
    own_partner.wait_send()

    def drain_1(j, _):
        mod_copy(j).wait_send()
        return 0

    def drain_2(j, _):
        tot_copy(j).wait_send()
        return 0

    lax.fori_loop(1, n_sp, drain_1, 0)
    lax.fori_loop(1, n_tp, drain_2, 0)


def ring_position(index, n_z, n_x):
    z, x = index // n_x, index % n_x
    back = n_z * (n_x - 1) + n_z - 1 - z
    out = z * (n_x - 1) + jnp.where(z % 2 == 0, x - 1, n_x - 1 - x)
    return jnp.where(x == 0, back, out)


def ring_index(place, n_z, n_x):
    r, k = place // (n_x - 1), place % (n_x - 1)
    out = r * n_x + jnp.where(r % 2 == 0, 1 + k, n_x - 1 - k)
    back = (n_z - 1 - (place - n_z * (n_x - 1))) * n_x
    return jnp.where(place >= n_z * (n_x - 1), back, out)


def attend_kernel(
    n_sp, n_tp, n_x, q_heads, k_heads, chunks,
    qz, kv, call, lift, wo,
    by_rows, wo_all,
    right, left, m_ref, acc, att,
    s_kv, r_kv, s_wy, r_wy, s_wp, r_wp, s_a, r_a, loc,
):
    me = lax.axis_index("sp")
    t = lax.axis_index("tp")
    n_y = n_tp // 2
    y, c = t // 2, t % 2
    partner = y * 2 + 1 - c
    half = n_sp // 2
    if n_x > 1:
        n_z = n_sp // n_x
        place = ring_position(me, n_z, n_x)
        nxt = ring_index(lax.rem(place + 1, n_sp), n_z, n_x)
        prv = ring_index(lax.rem(place + n_sp - 1, n_sp), n_z, n_x)
    else:
        nxt, prv = lax.rem(me + 1, n_sp), lax.rem(me + n_sp - 1, n_sp)
    barrier = pltpu.get_barrier_semaphore()
    for peer in (nxt, prv):
        pl.semaphore_signal(barrier, inc=1, device_id=(peer, t), device_id_type=pl.DeviceIdType.MESH)

    def greet(j, _):
        pl.semaphore_signal(barrier, inc=1, device_id=(me, lax.rem(t + j, n_tp)), device_id_type=pl.DeviceIdType.MESH)
        return 0

    lax.fori_loop(1, n_tp, greet, 0)
    pl.semaphore_wait(barrier, 2 + n_tp - 1)

    length = kv.shape[0]
    mid = length // 2

    def hop(src, dst, direction, i):
        return remote(src, dst, s_kv.at[direction, i], r_kv.at[direction, i], nxt if direction == 0 else prv, t)

    def sends(i, source_r, source_l):
        return (hop(source_r, right.at[i], 0, i), hop(source_l, left.at[i], 1, i))

    def last_sends(source_r, source_l):
        return (
            hop(source_r.at[pl.ds(0, mid)], right.at[half, pl.ds(0, mid)], 0, half),
            hop(source_l.at[pl.ds(mid, mid)], right.at[half, pl.ds(mid, mid)], 1, half),
        )

    opening = sends(1, kv, kv)
    for copy in opening:
        copy.start()
    own_w = pltpu.make_async_copy(wo, wo_all.at[t], loc.at[0])
    own_w.start()

    def w_y(k, ch):
        other = lax.rem(y + k, n_y)
        return remote(wo.at[ch], wo_all.at[t, ch], s_wy.at[k, ch], r_wy.at[t, ch], me, other * 2 + c)

    def w_own(ch):
        return remote(wo.at[ch], wo_all.at[t, ch], s_wp.at[0, ch], r_wp.at[t, ch], me, partner)

    def w_fwd(k, ch):
        other = lax.rem(y + n_y - k, n_y)
        near = other * 2 + c
        return remote(wo_all.at[near, ch], wo_all.at[near, ch], s_wp.at[k, ch], r_wp.at[near, ch], me, partner)

    for ch in range(chunks):
        for k in range(1, n_y):
            w_y(k, ch).start()
    for ch in range(chunks):
        w_own(ch).start()

    def forward_weight(ch):
        for k in range(1, n_y):
            other = lax.rem(y + n_y - k, n_y)
            near = other * 2 + c
            pltpu.make_async_copy(wo_all.at[near, ch], wo_all.at[near, ch], r_wy.at[near, ch]).wait()
            w_fwd(k, ch).start()

    k_width = kv.shape[1] // 2
    group = q_heads // k_heads
    tile = min(256, length)
    tiles = length // tile

    def attend(blocks, start, lifted):
        def one(head, _):
            lane = pl.multiple_of(head // (2 * group) * 128, 128)
            extra = lift[head]
            spans = [pl.ds(i * tile, tile) for i in range(tiles)]
            olds = [] if start else [m_ref[head, span, :] for span in spans]
            keys = [block[:, pl.ds(lane, 128)] for block in blocks]
            values = [block[:, pl.ds(pl.multiple_of(k_width + lane, 128), 128)] for block in blocks]
            values = [jnp.concatenate([v, jnp.ones_like(v)], axis=1) for v in values]
            scores = [
                [
                    lax.dot_general(
                        qz[head, span, :], k, (((1,), (1,)), ((), ())), preferred_element_type=F32
                    )
                    for k in keys
                ]
                for span in spans
            ]
            tops, outs = [], []
            for i in range(tiles):
                peaks = [jnp.max(s, axis=-1, keepdims=True) for s in scores[i]]
                if lifted:
                    peaks[-1] = peaks[-1] + extra
                top = functools.reduce(jnp.maximum, peaks)
                if not start:
                    top = jnp.maximum(olds[i][:, 0:1], top)
                out = None
                for pos, s in enumerate(scores[i]):
                    base = top - extra if lifted and pos == len(blocks) - 1 else top
                    term = dot(jnp.exp(s - base).astype(BF16), values[pos])
                    out = term if out is None else out + term
                wide = jnp.broadcast_to(top, (tile, 128))
                if not start:
                    f = jnp.exp(olds[i] - wide)
                    out = acc[head, spans[i], :] * jnp.concatenate([f, f], axis=1) + out
                tops.append(wide)
                outs.append(out)
            for i in range(tiles):
                m_ref[head, spans[i], :] = tops[i]
                acc[head, spans[i], :] = outs[i]
            return 0

        lax.fori_loop(0, q_heads, one, 0)

    attend([kv], True, False)

    def wait_pair(i):
        for copy in sends(i, kv, kv):
            copy.wait_recv()

    def step(i, _):
        wait_pair(i)
        for copy in sends(i + 1, right.at[i], left.at[i]):
            copy.start()
        attend([right.at[i], left.at[i]], False, False)
        forward_weight(i - 1)
        return 0

    lax.fori_loop(1, half - 1, step, 0)
    wait_pair(half - 1)
    closing = last_sends(right.at[half - 1], left.at[half - 1])
    for copy in closing:
        copy.start()
    attend([right.at[half - 1], left.at[half - 1]], False, False)
    for ch in range(half - 2, chunks):
        forward_weight(ch)
    for copy in closing:
        copy.wait_recv()
    attend([right.at[half], call], False, True)

    low_half = lax.broadcasted_iota(jnp.int32, (length, 128), 1) < HEAD
    per = length // n_tp

    def normal(head):
        return acc[head, :, :128] / acc[head, :, 128:]

    for two in range(q_heads // 2):
        parts = []
        for head in (2 * two, 2 * two + 1):
            o = normal(head)
            if (head // group) % 2 != head % 2:
                o = pltpu.roll(o, HEAD, 1)
            parts.append(o)
        both = jnp.where(low_half, parts[0], parts[1]).astype(BF16)
        for j in range(n_tp):
            att[j, :, two * 128 : two * 128 + 128] = both[j * per : (j + 1) * per, :]

    def a_copy(j):
        to = lax.rem(t + j, n_tp)
        return remote(att.at[to], by_rows.at[t], s_a.at[j], r_a.at[t], me, to)

    for j in range(1, n_tp):
        a_copy(j).start()
    own_a = pltpu.make_async_copy(att.at[t], by_rows.at[t], loc.at[1])
    own_a.start()
    own_a.wait()
    for j in range(1, n_tp):
        src = lax.rem(t + j, n_tp)
        pltpu.make_async_copy(by_rows.at[src], by_rows.at[src], r_a.at[src]).wait()
    own_w.wait()
    for ch in range(chunks):
        for k in range(n_y):
            far = lax.rem(y + n_y - k, n_y) * 2 + 1 - c
            pltpu.make_async_copy(wo_all.at[far, ch], wo_all.at[far, ch], r_wp.at[far, ch]).wait()
        for k in range(1, n_y):
            w_y(k, ch).wait_send()
            w_fwd(k, ch).wait_send()
        w_own(ch).wait_send()
    for j in range(1, n_tp):
        a_copy(j).wait_send()

    def drain(i, _):
        for copy in sends(i, kv, kv):
            copy.wait_send()
        return 0

    lax.fori_loop(1, half, drain, 0)
    for copy in closing:
        copy.wait_send()


def rotary_tables(offset, count):
    position = offset + jnp.arange(count, dtype=jnp.int32)
    grid_row = (position // GRID).astype(F32)
    grid_column = (position % GRID).astype(F32)
    quarter = HEAD // 4
    frequency = ROTARY_BASE ** (-jnp.arange(quarter, dtype=F32) / quarter)
    angles = jnp.concatenate([grid_row[:, None] * frequency, grid_column[:, None] * frequency], axis=1)
    sign = jnp.where(jnp.arange(HEAD) % 2 == 0, -1.0, 1.0)
    cos_t, sin_t = jnp.repeat(jnp.cos(angles), 2, axis=1), jnp.repeat(jnp.sin(angles), 2, axis=1) * sign
    return jnp.tile(cos_t, (1, 2)), jnp.tile(sin_t, (1, 2))


def shards(
    n_sp, n_tp, n_x,
    latent, context, conditioning, context_conditioning, shift_weight, scale_weight, gate_weight,
    norm_gain, query_weight, key_weight, value_weight, query_gain, key_gain, context_lift, output_weight,
):
    k_heads = key_weight.shape[1] // HEAD
    q_heads = query_weight.shape[1] // HEAD
    if k_heads % 2:
        key_weight = jnp.pad(key_weight, ((0, 0), (0, HEAD)))
        value_weight = jnp.pad(value_weight, ((0, 0), (0, HEAD)))
    rows, model = latent.shape
    length = rows * n_tp
    k_width = key_weight.shape[1]
    c_rows = context.shape[0]
    part_width = shift_weight.shape[1]
    cos_t, sin_t = rotary_tables(lax.axis_index("sp") * length, length)
    vmem = pl.BlockSpec(memory_space=VMEM)
    dma = pltpu.SemaphoreType.DMA
    hbm = pl.BlockSpec(memory_space=pltpu.HBM)
    qz, kv, call, gate = pl.pallas_call(
        functools.partial(project_kernel, n_sp, n_tp, q_heads, k_heads),
        name="project",
        out_shape=(
            jax.ShapeDtypeStruct((q_heads, n_tp, rows, 128), BF16),
            jax.ShapeDtypeStruct((n_tp, rows, 2 * k_width), BF16),
            jax.ShapeDtypeStruct((n_sp, c_rows, 2 * k_width), BF16),
            jax.ShapeDtypeStruct((1, model), F32),
        ),
        in_specs=[hbm, hbm, vmem, vmem, hbm, hbm, hbm, vmem, hbm, hbm, hbm, vmem, vmem, vmem, vmem],
        out_specs=(vmem,) * 4,
        scratch_shapes=[
            VMEM(latent.shape, BF16), VMEM(context.shape, BF16),
            VMEM(shift_weight.shape, BF16), VMEM(scale_weight.shape, BF16), VMEM(gate_weight.shape, BF16),
            VMEM(query_weight.shape, BF16), VMEM(key_weight.shape, BF16), VMEM(value_weight.shape, BF16),
            VMEM((n_tp, rows, model), BF16),
            VMEM((c_rows, 2 * k_width), BF16),
            VMEM((8, part_width), F32),
            VMEM((8, part_width), F32),
            VMEM((n_sp, 8, part_width), F32),
            VMEM((n_tp, 8, part_width), F32),
            VMEM((8, model), F32),
            dma((n_sp,)), dma((n_sp,)), dma((n_tp,)), dma((n_tp,)),
            dma((n_tp,)), dma((n_tp,)), dma, dma((n_tp,)), dma((n_tp,)),
            dma((n_sp,)), dma((n_sp,)), dma((8,)),
        ],
        compiler_params=pltpu.CompilerParams(
            collective_id=0, has_side_effects=True, vmem_limit_bytes=67043328
        ),
    )(
        latent, context, conditioning[None], context_conditioning[None],
        shift_weight, scale_weight, gate_weight, norm_gain[None],
        query_weight, key_weight, value_weight,
        jnp.tile(query_gain, 2)[None], jnp.tile(key_gain, 2)[None],
        cos_t.reshape(n_tp, rows, 128), sin_t.reshape(n_tp, rows, 128),
    )
    chunks = max(n_sp // 2, 2)
    o_rows = output_weight.shape[0]
    by_rows, wo_all = pl.pallas_call(
        functools.partial(attend_kernel, n_sp, n_tp, n_x, q_heads, k_heads, chunks),
        name="attend",
        out_shape=(
            jax.ShapeDtypeStruct((n_tp, rows, q_heads * HEAD), BF16),
            jax.ShapeDtypeStruct((n_tp, chunks, o_rows // chunks, model), BF16),
        ),
        in_specs=[vmem, vmem, vmem, pl.BlockSpec(memory_space=pltpu.SMEM), vmem],
        out_specs=(vmem, pl.BlockSpec(memory_space=pl.ANY)),
        scratch_shapes=[
            VMEM((n_sp // 2 + 1, length, 2 * k_width), BF16),
            VMEM((n_sp // 2, length, 2 * k_width), BF16),
            VMEM((q_heads, length, 128), F32),
            VMEM((q_heads, length, 256), F32),
            VMEM((n_tp, rows, q_heads * HEAD), BF16),
            dma((2, n_sp)), dma((2, n_sp)),
            dma((n_tp, chunks)), dma((n_tp, chunks)), dma((n_tp, chunks)), dma((n_tp, chunks)),
            dma((n_tp,)), dma((n_tp,)), dma((2,)),
        ],
        compiler_params=pltpu.CompilerParams(
            collective_id=1, has_side_effects=True, vmem_limit_bytes=56 * 1024 * 1024
        ),
    )(
        qz.reshape(q_heads, length, 128), kv.reshape(length, 2 * k_width),
        call.reshape(n_sp * c_rows, 2 * k_width), context_lift,
        output_weight.reshape(chunks, o_rows // chunks, model),
    )
    projection = jnp.dot(
        jnp.transpose(by_rows, (1, 0, 2)).reshape(rows, n_tp * o_rows),
        wo_all.reshape(n_tp * o_rows, model),
        preferred_element_type=F32,
    )
    return (latent.astype(F32) + gate * projection).astype(BF16)


def solution(mesh):
    try:
        n_x = len({d.coords[0] for d in mesh.devices[:, 0]})
    except AttributeError:
        n_x = 1
    n_sp, n_tp = mesh.shape["sp"], mesh.shape["tp"]
    if n_x < 2 or n_sp % n_x or (n_sp // n_x) % 2:
        n_x = 1
    in_specs = (
        P(("sp", "tp"), None), P("sp", None), P("sp"), P("sp"),
        P("sp", "tp"), P("sp", "tp"), P("sp", "tp"), P(),
        P(None, "tp"), P(None, "tp"), P(None, "tp"), P(), P(), P("tp"), P("tp", None),
    )
    body = functools.partial(shards, n_sp, n_tp, n_x)
    return jax.shard_map(body, mesh=mesh, in_specs=in_specs, out_specs=P(("sp", "tp"), None), check_vma=False)
```

profile of v0, /device:TPU:1, one launch (start us, length us, event | category | flops | bytes accessed | tf_op | source)
XLA Modules:
  0.0 115.8 jit_solution(629375800311027166)
XLA Ops:
  0.0 0.7 tile.14
  0.7 0.6 broadcast_in_dim_tile.6.q_gain
  1.3 0.7 tile.30
  1.9 0.6 broadcast_in_dim_tile.7.k_gain
  2.5 0.1 broadcast_multiply_fusion.2
  2.6 0.2 fusion.2
  2.9 0.1 reshape.100
  3.0 0.1 broadcast_multiply_fusion
  3.1 0.1 tile.35
  3.2 0.8 copy.17.sin_t
  4.1 0.1 tile.31
  4.2 0.1 tile.33
  4.3 0.8 copy.16.cos_t
  5.2 32.0 %project.1 = (bf16[8,4,128,128]{3,2,1,0:T(8,128)(2,1)}, bf16[4,128,512]{2,1,0:T(8,128)(2,1)}, bf16[8,64,512]{2,1,0:T(8,128)(2,1)}, f32[1,2048]{1,0:T(1,128)}) custom-call(bf16[128,2048]{1,0:T(8,128)(2,1)} %latent_h.1, bf16[64,2048]{1,0:T(8,128)(2,1)} %context_h.1, f32[1,256]{1,0:T(1,128)} %bitcast.30, f32[1,256]{1,0:T(1,128)} %bitcast.31, ...), custom_call_target="tpu_custom_call" | custom-call | tf_op jit(solution)/shard_map/project/pallas_call | solution.py:499
  37.1 71.6 %attend.1 = (bf16[4,128,512]{2,1,0:T(8,128)(2,1)}, bf16[4,4,128,2048]{3,2,1,0:T(8,128)(2,1)}) custom-call(bf16[8,512,128]{2,1,0:T(8,128)(2,1)} %bitcast.24, bf16[512,512]{1,0:T(8,128)(2,1)} %bitcast.25, bf16[512,512]{1,0:T(8,128)(2,1)} %bitcast.26, f32[8]{0:T(128)} %lift.1, bf16[4,128,2048]{2,1,0:T(8,128)(2,1)} %bitcast.23), custom_call_target="tpu_custom_call" | custom-call | tf_op jit(solution)/shard_map/attend/pallas_call | solution.py:537
  108.8 1.3 %copy.18 = bf16[128,4,512]{0,2,1:T(8,128)(2,1)S(1)} copy(bf16[128,4,512]{2,0,1:T(8,128)(2,1)} %bitcast.27) | data formatting | bytes 1048576 | tf_op jit(solution)/shard_map/transpose | solution.py:565
  110.1 5.7 %fusion.1 = bf16[128,2048]{1,0:T(8,128)(2,1)} fusion(bf16[128,2048]{0,1:T(8,128)(2,1)S(1)} %bitcast.22, bf16[2048,2048]{1,0:T(8,128)(2,1)} %bitcast.21, bf16[128,2048]{1,0:T(8,128)(2,1)} %latent_h.1, f32[2048]{0:T(1024)} %bitcast.29), kind=kOutput, calls=%fused_computation.2 | convolution fusion | flops 1074790400 | bytes 9969664 | tf_op jit(solution)/shard_map/dot_general | solution.py:564
  (7 shorter events, 0.2 us)
where the time goes:
time: 116 us
  Pallas kernels  104 us (90%)
  local copies, waits for them, and re-layouts  5.98 us (5%)
  matrix products  5.65 us (5%)
    pallas_call x1, Pallas kernels, shards(): pl.pallas_call(functools.partial(attend_kernel, n_sp, n_tp, n_x, q_heads,...  71.6 us
    pallas_call x1, Pallas kernels, shards(): pl.pallas_call(functools.partial(project_kernel, n_sp, n_tp, q_heads, k_h...  32 us
    dot_general x1, matrix products, shards(): jnp.dot(jnp.transpose(by_rows, (1, 0, 2)).reshape(rows, n_tp * o_rows), w...  5.65 us

commit v1 on v0

v1 whole, which is shorter than its diff:
```python
import functools
import math

import jax
import jax.numpy as jnp
from jax import lax
from jax.experimental import pallas as pl
from jax.experimental.pallas import tpu as pltpu
from jax.sharding import PartitionSpec as P

HEAD = 64
GRID = 64
EPSILON = 1e-06
ROTARY_BASE = 10000.0
F32 = jnp.float32
BF16 = jnp.bfloat16
VMEM = pltpu.VMEM
TILE = 256
ONES = 16
NT_DIMS = (((1,), (1,)), ((), ()))


def dot(a, b):
    return jnp.dot(a, b, preferred_element_type=F32)


def dot_nt(a, b):
    return lax.dot_general(a, b, NT_DIMS, preferred_element_type=F32)


def remote(src, dst, send, recv, sp, tp):
    return pltpu.make_async_remote_copy(
        src_ref=src,
        dst_ref=dst,
        send_sem=send,
        recv_sem=recv,
        device_id=(sp, tp),
        device_id_type=pl.DeviceIdType.MESH,
    )


def loop(low, high, body):
    def step(i, _):
        body(i)
        return 0

    lax.fori_loop(low, high, step, 0)


def fused_kernel(
    n_sp, n_tp, groups, w_chunks, l_chunks,
    latent_h, context_h, cond, ctx_cond, shift_h, scale_h, gate_h, gain,
    wq_h, wk_h, wv_h, q_gain, k_gain, lift, wo_h,
    out,
    lat, ctxp, shift_w, scale_w, gate_w, wq, wk, wv, w_t, wo_all,
    part, total, recv1, recv2, mods, rows8, hid, cos_t, sin_t,
    qst, kst, vst, cst, qin, kin, vin, cin, kcx, vcx, qbd,
    sa, sb, m_ref, acc, ost, att_t, att,
    loads, s1, r1, s2, r2, sy, ry, sfw, rp,
    sq, rq, sk, rk, sv, rv, sc, rc,
    swy, rwy, swx, rwx, swp, rwp, swo, rwo, s_out, r_out,
):
    me = lax.axis_index("sp")
    t = lax.axis_index("tp")
    n_y = n_tp // 2
    y, c = t // 2, t % 2
    partner = y * 2 + 1 - c
    halves = n_sp // groups
    half, g = me // groups, me % groups
    rows, model = lat.shape[1], lat.shape[2]
    per_tile = TILE // rows
    n_tiles = rows * n_tp // TILE
    y_per = per_tile // 2
    own_block = t // per_tile
    c_rows = context_h.shape[0]
    width = total.shape[1]

    def block(k):
        return lax.rem(own_block + k, n_tiles)

    fetch = [
        pltpu.make_async_copy(src, dst, loads.at[i])
        for i, (src, dst) in enumerate(
            (
                (latent_h, lat.at[t]), (shift_h, shift_w), (scale_h, scale_w), (gate_h, gate_w),
                (wq_h, wq), (wk_h, wk), (wv_h, wv),
                (context_h, ctxp.at[pl.ds(0, c_rows)]), (wo_h, wo_all.at[t]),
            )
        )
    ]
    for copy in fetch:
        copy.start()
    barrier = pltpu.get_barrier_semaphore()

    def greet(sp, tp):
        pl.semaphore_signal(barrier, inc=1, device_id=(sp, tp), device_id_type=pl.DeviceIdType.MESH)

    loop(1, n_sp, lambda j: greet(lax.rem(me + j, n_sp), t))

    def greet_half(j):
        loop(1, n_tp, lambda i: greet(half * groups + j, lax.rem(t + i, n_tp)))

    loop(0, groups, greet_half)
    pl.semaphore_wait(barrier, n_sp - 1 + groups * (n_tp - 1))

    piece = rows // l_chunks
    fetch[0].wait()

    def y_copy(k, ch):
        other = lax.rem(y + k, n_y)
        part_of = lat.at[t, pl.ds(ch * piece, piece)]
        return remote(part_of, part_of, sy.at[k, ch], ry.at[t, ch], me, other * 2 + c)

    def y_start(ch):
        loop(1, n_y, lambda k: y_copy(k, ch).start())

    early = (l_chunks + 1) // 2
    for ch in range(early):
        y_start(ch)
    own_partner = remote(lat.at[t], lat.at[t], sfw.at[0, 0], rp.at[t, 0], me, partner)
    own_partner.start()

    shape8 = (8, cond.shape[1])
    row8 = lax.broadcasted_iota(jnp.int32, shape8, 0)
    a = jnp.broadcast_to(cond[...] / (1.0 + jnp.exp(-cond[...])), shape8)
    b = jnp.broadcast_to(ctx_cond[...] / (1.0 + jnp.exp(-ctx_cond[...])), shape8)
    first = jnp.where(row8 == 0, a, jnp.where(row8 == 1, b, 0.0)).astype(BF16)
    second = jnp.where(row8 == 2, a, jnp.where(row8 == 3, b, 0.0)).astype(BF16)
    third = jnp.where(row8 == 4, a, 0.0).astype(BF16)
    for copy in fetch[1:4]:
        copy.wait()
    mine = dot(first, shift_w[...]) + dot(second, scale_w[...]) + dot(third, gate_w[...])
    part[...] = mine
    recv1[me] = mine

    def mod_copy(j):
        return remote(part, recv1.at[me], s1.at[j], r1.at[me], lax.rem(me + j, n_sp), t)

    loop(1, n_sp, lambda j: mod_copy(j).start())

    for copy in fetch[4:7]:
        copy.wait()

    def turn_weights(i):
        span = pl.ds(pl.multiple_of(i * TILE, TILE), TILE)
        q_rows, k_rows, v_rows = (jnp.transpose(w[span, :]) for w in (wq, wk, wv))
        for j in range(groups):
            w_t[j, 0 : 2 * HEAD, span] = q_rows[2 * HEAD * j : 2 * HEAD * (j + 1), :]
            w_t[j, 2 * HEAD : 3 * HEAD, span] = k_rows[HEAD * j : HEAD * (j + 1), :]
            w_t[j, 3 * HEAD : 4 * HEAD, span] = v_rows[HEAD * j : HEAD * (j + 1), :]

    n_turns = model // TILE
    loop(0, n_turns // 2, turn_weights)

    def mod_wait(j):
        src = lax.rem(me + j, n_sp)
        pltpu.make_async_copy(recv1.at[src], recv1.at[src], r1.at[src]).wait()

    loop(1, n_sp, mod_wait)
    summed = lax.fori_loop(1, n_sp, lambda j, s: s + recv1[j], recv1[0])
    total[...] = summed
    recv2[t] = summed

    def tot_copy(j):
        return remote(total, recv2.at[t], s2.at[j], r2.at[t], me, lax.rem(t + j, n_tp))

    loop(1, n_tp, lambda j: tot_copy(j).start())
    for ch in range(early, l_chunks):
        y_start(ch)

    loop(n_turns // 2, n_turns, turn_weights)

    channel = lax.broadcasted_iota(jnp.int32, (HEAD, TILE), 0)
    lane = lax.broadcasted_iota(jnp.int32, (HEAD, TILE), 1)
    quarter = HEAD // 4
    power = ((channel // 2) % quarter).astype(F32)
    frequency = jnp.exp(power * (-math.log(ROTARY_BASE) / quarter))
    even = channel % 2 == 0

    def tables(i):
        position = (me * n_tiles + i) * TILE + lane
        place = jnp.where(channel < HEAD // 2, position // GRID, position % GRID)
        angle = place.astype(F32) * frequency
        cos_t[i] = jnp.cos(angle)
        sine = jnp.sin(angle)
        sin_t[i] = jnp.where(even, -sine, sine)

    loop(0, n_tiles, tables)

    def blank(i):
        qbd[i] = jnp.zeros(qbd.shape[1:], BF16)

    loop(0, qbd.shape[0], blank)

    def ones(ref, i):
        ref[i, HEAD:, :] = jnp.ones((ONES, TILE), BF16)

    loop(0, vin.shape[0], lambda i: ones(vin, i))
    loop(0, vcx.shape[0], lambda i: ones(vcx, i))

    def tot_wait(j):
        src = lax.rem(t + j, n_tp)
        pltpu.make_async_copy(recv2.at[src], recv2.at[src], r2.at[src]).wait()

    loop(1, n_tp, tot_wait)
    for j in range(n_tp):
        mods[:, j * width : (j + 1) * width] = recv2[j]
    for i, (shift_row, scale_row) in enumerate(((0, 2), (1, 3))):
        factor = gain[...] * (1.0 + mods[scale_row : scale_row + 1, :])
        rows8[2 * i] = jnp.broadcast_to(factor, (8, model))
        rows8[2 * i + 1] = jnp.broadcast_to(mods[shift_row : shift_row + 1, :], (8, model))

    step_rows = 32

    def hidden_of(x, which):
        x = x.astype(F32)
        inv = lax.rsqrt(jnp.mean(x * x, axis=-1, keepdims=True) + EPSILON)
        x = (x * inv).reshape(x.shape[0] // 8, 8, model)
        return (x * rows8[2 * which][None] + rows8[2 * which + 1][None]).reshape(-1, model)

    q_gains = jnp.broadcast_to(q_gain[...], (HEAD, TILE))
    k_gains = jnp.broadcast_to(k_gain[...], (HEAD, TILE))

    def norm(v, gains):
        mean = jnp.mean(v * v, axis=0, keepdims=True)
        return v * lax.rsqrt(mean + EPSILON) * gains

    def turn(v, cos_v, sin_v):
        v3 = v.reshape(HEAD // 8, 8, TILE)
        pairs = lax.broadcasted_iota(jnp.int32, v3.shape, 1) % 2 == 0
        swapped = jnp.where(pairs, pltpu.roll(v3, 7, 1), pltpu.roll(v3, 1, 1)).reshape(HEAD, TILE)
        return v * cos_v + swapped * sin_v

    def q_copy(bk, j, to):
        return remote(qst.at[bk, j], qin.at[g, bk], sq.at[bk, to], rq.at[g, bk], half * groups + j, t)

    def kv_copies(bk, n):
        j = lax.rem(g + n, groups)
        to = lax.rem(half + n // groups, halves) * groups + j
        slot = me * n_tiles + bk
        return (
            remote(kst.at[bk, j], kin.at[slot], sk.at[bk, n], rk.at[me, bk], to, t),
            remote(
                vst.at[bk, j], vin.at[slot, pl.ds(0, HEAD)], sv.at[bk, n], rv.at[me, bk], to, t
            ),
        )

    def project(bk):
        def hide(i):
            start = i * step_rows
            x = lat[bk * per_tile + start // rows, pl.ds(start % rows, step_rows), :]
            hid[pl.ds(pl.multiple_of(start, step_rows), step_rows), :] = hidden_of(x, 0).astype(BF16)

        loop(0, TILE // step_rows, hide)
        cos_v, sin_v = cos_t[bk], sin_t[bk]
        order = [lax.rem(g + n, groups) for n in list(range(1, groups)) + [0]]
        ahead = dot_nt(w_t[order[0]], hid[...])
        for place, j in enumerate(order):
            z = ahead
            if place + 1 < groups:
                ahead = dot_nt(w_t[order[place + 1]], hid[...])
            for i in range(2):
                q = turn(norm(z[HEAD * i : HEAD * (i + 1)], q_gains), cos_v, sin_v)
                qst[bk, j, i] = (q.astype(BF16).astype(F32) * HEAD ** (-0.5)).astype(BF16)
            k = turn(norm(z[2 * HEAD : 3 * HEAD], k_gains), cos_v, sin_v)
            k = jnp.concatenate([k[:, :128], k[:, 128:]], axis=0)
            kst[bk, j] = jnp.transpose(k).astype(BF16)
            vst[bk, j] = z[3 * HEAD :].astype(BF16)
            n = (place + 1) % groups
            if n:
                q_copy(bk, j, n).start()
                for copy in kv_copies(bk, n):
                    copy.start()
        qin[g, bk] = qst[bk, g]
        kin[me * n_tiles + bk] = kst[bk, g]
        vin[me * n_tiles + bk, 0:HEAD, :] = vst[bk, g]

        def cross(n):
            for copy in kv_copies(bk, n):
                copy.start()

        loop(groups, n_sp, cross)

    def y_near(other):
        return other * 2 + c, other * 2 + 1 - c

    def forward(other, ch):
        near, _ = y_near(other)
        part_of = lat.at[near, pl.ds(ch * piece, piece)]
        return remote(part_of, part_of, sfw.at[1 + other, ch], rp.at[near, ch], me, partner)

    def take(other):
        near, far = y_near(other)
        for ch in range(l_chunks):
            part_of = lat.at[near, pl.ds(ch * piece, piece)]
            pltpu.make_async_copy(part_of, part_of, ry.at[near, ch]).wait()
            forward(other, ch).start()
        for ch in range(l_chunks):
            part_of = lat.at[far, pl.ds(ch * piece, piece)]
            pltpu.make_async_copy(part_of, part_of, rp.at[far, ch]).wait()

    pltpu.make_async_copy(lat.at[partner], lat.at[partner], rp.at[partner, 0]).wait()
    if y_per > 1:
        loop(1, y_per, lambda o: take(own_block * y_per + lax.rem(y % y_per + o, y_per)))
    project(block(0))

    fetch[7].wait()
    c_lane = lax.broadcasted_iota(jnp.int32, (HEAD, 128), 1)

    def hide_context(i):
        span = pl.ds(pl.multiple_of(i * step_rows, step_rows), step_rows)
        row = i * step_rows + lax.broadcasted_iota(jnp.int32, (step_rows, model), 0)
        keep = row < c_rows
        h = hidden_of(jnp.where(keep, ctxp[span, :].astype(F32), 0.0), 1)
        hid[span, :] = jnp.where(keep, h, 0.0).astype(BF16)

    loop(0, 128 // step_rows, hide_context)
    for j in range(groups):
        z = dot_nt(w_t[j, 2 * HEAD :], hid[0:128, :])
        k = norm(z[:HEAD], k_gains[:, :128])
        cst[j] = jnp.where(c_lane < HEAD, k, pltpu.roll(z[HEAD:], HEAD, 1)).astype(BF16)

    def c_copy(n):
        to = lax.rem(half + n // groups, halves) * groups + lax.rem(g + n, groups)
        return remote(cst.at[lax.rem(g + n, groups)], cin.at[me], sc.at[n], rc.at[me], to, t)

    loop(1, n_sp, lambda n: c_copy(n).start())
    cin[me] = cst[g]

    fetch[8].wait()
    side = me % 2
    across = me + 1 - 2 * side

    def w_y(k, ch):
        other = lax.rem(y + k, n_y)
        ref = wo_all.at[t, side, ch]
        return remote(ref, ref, swy.at[k, ch], rwy.at[t, ch], me, other * 2 + c)

    def w_x(other, ch):
        near, _ = y_near(other)
        ref = wo_all.at[near, side, ch]
        return remote(ref, ref, swx.at[other, ch], rwx.at[near, ch], across, t)

    def w_p(other, ch, second):
        near, _ = y_near(other)
        ref = wo_all.at[near, 1 - side if second else side, ch]
        return remote(ref, ref, swp.at[other, ch, second], rwp.at[near, ch, second], me, partner)

    w_own = remote(wo_all.at[t], wo_all.at[t], swo, rwo, me, partner)

    def forward_y(ch):
        def one(k):
            other = lax.rem(y + n_y - k, n_y)
            near, _ = y_near(other)
            ref = wo_all.at[near, side, ch]
            pltpu.make_async_copy(ref, ref, rwy.at[near, ch]).wait()
            w_x(other, ch).start()
            w_p(other, ch, 0).start()

        loop(1, n_y, one)

    def forward_x(ch):
        def one(k):
            other = lax.rem(y + n_y - k, n_y)
            near, _ = y_near(other)
            ref = wo_all.at[near, 1 - side, ch]
            pltpu.make_async_copy(ref, ref, rwx.at[near, ch]).wait()
            w_p(other, ch, 1).start()

        loop(1, n_y, one)

    for ch in range(w_chunks):
        loop(1, n_y, lambda k, ch=ch: w_y(k, ch).start())
    w_own.start()

    for k in range(1, n_tiles):
        loop(0, y_per, lambda o, k=k: take(block(k) * y_per + o))
        project(block(k))

    def wait_kv(d, k, low):
        bk = block(k)

        def one(i):
            s = lax.rem(half + d, halves) * groups + lax.rem(g + i, groups)
            slot = s * n_tiles + bk
            pltpu.make_async_copy(kin.at[slot], kin.at[slot], rk.at[s, bk]).wait()
            ref = vin.at[slot, pl.ds(0, HEAD)]
            pltpu.make_async_copy(ref, ref, rv.at[s, bk]).wait()

        loop(low, groups, one)

    def wait_own(k):
        bk = block(k)

        def one(i):
            j = lax.rem(g + i, groups)
            pltpu.make_async_copy(qin.at[j, bk], qin.at[j, bk], rq.at[j, bk]).wait()

        loop(1, groups, one)
        wait_kv(0, k, 1)

        def spread(j):
            for i in range(2):
                q = qin[j, bk, i]
                slot = (j * n_tiles + bk) * 2 + i
                qbd[slot, 0:HEAD, 0:TILE] = q
                qbd[slot, HEAD:, TILE:] = q

        loop(0, groups, spread)

    def wait_cross(d, k):
        wait_kv(d, k, 0)

    def wait_context():
        def one(j):
            s = lax.rem(me + j, n_sp)
            pltpu.make_async_copy(cin.at[s], cin.at[s], rc.at[s]).wait()

        loop(1, n_sp, one)
        per = 128 // c_rows
        for u in range(kcx.shape[0]):
            keys, values = [], []
            for m in (2 * u, 2 * u + 1):
                k = v = jnp.zeros((HEAD, 128), F32)
                for i in range(per):
                    at = i * c_rows
                    both = cin[m * per + i].astype(F32)
                    keep = (c_lane >= at) & (c_lane < at + c_rows)
                    k = jnp.where(keep, pltpu.roll(both, at, 1) if at else both, k)
                    back = (at - HEAD) % 128
                    v = jnp.where(keep, pltpu.roll(both, back, 1) if back else both, v)
                keys.append(k)
                values.append(v)
            kcx[u] = jnp.transpose(jnp.concatenate(keys, axis=0)).astype(BF16)
            vcx[u, 0:HEAD, :] = jnp.concatenate(values, axis=1).astype(BF16)

    def slabs(d, k):
        base = lax.rem(half + d, halves) * groups
        slots = [(base + i) * n_tiles + block(k) for i in range(groups)]
        return [(kin, vin, slot, False) for slot in slots]

    context = [(kcx, vcx, u, True) for u in range(kcx.shape[0])]

    def out_copy(bk, j, p):
        return remote(
            ost.at[bk, j, p], att_t.at[t, g], s_out.at[bk, j, p], r_out.at[t, g],
            half * groups + j, bk * per_tile + p,
        )

    def sweep(k, blocks, start, final):
        bk = block(k)

        def slot_of(j, i):
            return (lax.rem(g + 1 + j, groups) * n_tiles + bk) * 2 + i

        def scores(j, i, dst):
            q = qbd[slot_of(j, i)]
            top = None
            for place, (keys, _, slot, lifted) in enumerate(blocks):
                s = dot(keys[slot], q)
                if lifted:
                    s = s + lift[g * 2 + i]
                dst[place] = s
                peak = jnp.max(s.reshape(s.shape[0] // 8, 8, s.shape[1]), axis=0)
                top = peak if top is None else jnp.maximum(top, peak)
            return top

        def soft(j, i, src, top):
            slot = slot_of(j, i)
            top = jnp.max(top, axis=0, keepdims=True)
            top = jnp.maximum(top[:, :TILE], top[:, TILE:])
            if not start:
                old = m_ref[slot, 0:1, :]
                top = jnp.maximum(old, top)
            wide = jnp.concatenate([top, top], axis=1)
            weights = []
            for place in range(len(blocks)):
                w = jnp.exp(src[place] - wide).astype(BF16)
                weights += [w[:, :TILE], w[:, TILE:]]
            values = jnp.concatenate([v[at] for _, v, at, _ in blocks], axis=1)
            o = dot(values, jnp.concatenate(weights, axis=0))
            if not start:
                o = acc[slot] * jnp.exp(old - top) + o
            if not final:
                acc[slot] = o
                m_ref[slot] = jnp.broadcast_to(top, (8, TILE))
                return
            o = (o[:HEAD] / o[HEAD : HEAD + 1]).astype(BF16)
            to = lax.rem(g + 1 + j, groups)
            for p in range(per_tile):
                ost[bk, to, p, i * HEAD : (i + 1) * HEAD, :] = o[:, p * rows : (p + 1) * rows]

        def pair(j, top):
            later = scores(j, 1, sb)
            soft(j, 0, sa, top)
            return later

        def body(j, top):
            later = pair(j, top)
            top = scores(j + 1, 0, sa)
            soft(j, 1, sb, later)
            if final:
                for p in range(per_tile):
                    out_copy(bk, lax.rem(g + 1 + j, groups), p).start()
            return top

        top = scores(0, 0, sa)
        top = lax.fori_loop(0, groups - 1, body, top)
        later = pair(groups - 1, top)
        soft(groups - 1, 1, sb, later)
        if final:
            for p in range(per_tile):
                if k:
                    out_copy(bk, g, p).start()
                else:

                    @pl.when(p != t % per_tile)
                    def _(p=p):
                        out_copy(bk, g, p).start()

            if k == 0:
                att_t[t, g] = ost[bk, g, t % per_tile]

    if n_tiles == 2 and halves == 2:
        wait_own(0)
        sweep(0, slabs(0, 0), True, False)
        wait_cross(1, 0)
        wait_context()
        sweep(0, slabs(1, 0) + context, False, False)
        wait_own(1)
        forward_y(0)
        sweep(1, slabs(0, 0) + slabs(0, 1) + context + slabs(1, 0), True, False)
        for ch in range(1, w_chunks - 1):
            forward_y(ch)
        forward_x(0)
        wait_cross(1, 1)
        sweep(1, slabs(1, 1), False, True)
        forward_y(w_chunks - 1)
        sweep(0, slabs(0, 1) + slabs(1, 1), False, True)
        for ch in range(1, w_chunks):
            forward_x(ch)
    else:
        for k in range(n_tiles):
            wait_own(k)
        wait_context()
        for k in range(n_tiles):
            own = [slab for i in range(n_tiles) for slab in slabs(0, i)]
            sweep(k, own + context, True, halves == 1)

        def further(d, final):
            for i in range(n_tiles):
                wait_cross(d, i)
            for k in range(n_tiles):
                sweep(k, [slab for i in range(n_tiles) for slab in slabs(d, i)], False, final)

        if halves > 1:
            loop(1, halves - 1, lambda d: further(d, False))
            further(halves - 1, True)
        for ch in range(w_chunks):
            forward_y(ch)
        for ch in range(w_chunks):
            forward_x(ch)

    ref = wo_all.at[partner]
    pltpu.make_async_copy(ref, ref, rwo).wait()

    def w_far(k):
        _, far = y_near(lax.rem(y + n_y - k, n_y))
        for ch in range(w_chunks):
            for second in range(2):
                ref = wo_all.at[far, 1 - side if second else side, ch]
                pltpu.make_async_copy(ref, ref, rwp.at[far, ch, second]).wait()

    loop(1, n_y, w_far)

    def out_wait(i):
        at = lax.rem(t * groups + g + i, n_tp * groups)
        ref = att_t.at[at // groups, at % groups]
        pltpu.make_async_copy(ref, ref, r_out.at[at // groups, at % groups]).wait()

    loop(1, n_tp * groups, out_wait)
    for i in range(n_tp):
        for j in range(groups):
            at = (i * groups + j) * 2 * HEAD
            att[:, at : at + 2 * HEAD] = jnp.transpose(att_t[i, j])
    n_out = 4
    wide = model // n_out
    for n in range(n_out):
        span = slice(n * wide, (n + 1) * wide)
        weight = wo_all[:, :, :, :, span].reshape(-1, wide)
        projection = dot(att[...], weight)
        out[:, span] = (lat[t, :, span].astype(F32) + mods[4:5, span] * projection).astype(BF16)

    own_partner.wait_send()
    w_own.wait_send()

    def drain_y(k):
        other = lax.rem(y + k, n_y)
        for ch in range(l_chunks):
            y_copy(k, ch).wait_send()
            forward(other, ch).wait_send()
        for ch in range(w_chunks):
            w_y(k, ch).wait_send()
            w_x(other, ch).wait_send()
            w_p(other, ch, 0).wait_send()
            w_p(other, ch, 1).wait_send()

    loop(1, n_y, drain_y)
    loop(1, n_sp, lambda j: mod_copy(j).wait_send())
    loop(1, n_tp, lambda j: tot_copy(j).wait_send())

    def drain_sp(n):
        c_copy(n).wait_send()
        for bk in range(n_tiles):
            for copy in kv_copies(bk, n):
                copy.wait_send()

    loop(1, n_sp, drain_sp)
    for bk in range(n_tiles):
        loop(1, groups, lambda n, bk=bk: q_copy(bk, lax.rem(g + n, groups), n).wait_send())

        def drain_out(j, bk=bk):
            for p in range(per_tile):

                @pl.when(jnp.logical_or(j != g, bk * per_tile + p != t))
                def _(p=p):
                    out_copy(bk, j, p).wait_send()

        loop(0, groups, drain_out)


def shards(
    n_sp, n_tp,
    latent, context, conditioning, context_conditioning, shift_weight, scale_weight, gate_weight,
    norm_gain, query_weight, key_weight, value_weight, query_gain, key_gain, context_lift, output_weight,
):
    k_heads = key_weight.shape[1] // HEAD
    q_heads = query_weight.shape[1] // HEAD
    rows, model = latent.shape
    c_rows = context.shape[0]
    o_rows = output_weight.shape[0]
    part_width = shift_weight.shape[1]
    assert q_heads == 2 * k_heads and n_sp % k_heads == 0 and n_sp % 2 == 0
    assert TILE % rows == 0 and rows * n_tp % TILE == 0 and 2 * c_rows <= 128
    groups = k_heads
    per_tile = TILE // rows
    n_tiles = rows * n_tp // TILE
    n_context = n_sp * c_rows // TILE
    w_chunks = 4 if o_rows >= 256 else 1
    l_chunks = 4 if rows >= 64 else 1
    most = groups * n_tiles * 2 + n_context
    n_q = groups * n_tiles * 2
    n_y = n_tp // 2
    vmem = pl.BlockSpec(memory_space=VMEM)
    dma = pltpu.SemaphoreType.DMA
    hbm = pl.BlockSpec(memory_space=pltpu.HBM)
    smem = pl.BlockSpec(memory_space=pltpu.SMEM)
    wo_shape = (2, w_chunks, o_rows // (2 * w_chunks), model)
    return pl.pallas_call(
        functools.partial(fused_kernel, n_sp, n_tp, groups, w_chunks, l_chunks),
        name="fused",
        out_shape=jax.ShapeDtypeStruct((rows, model), BF16),
        in_specs=[
            hbm, hbm, vmem, vmem, hbm, hbm, hbm, vmem, hbm, hbm, hbm, vmem, vmem, smem, hbm,
        ],
        out_specs=vmem,
        scratch_shapes=[
            VMEM((n_tp, rows, model), BF16), VMEM((128, model), BF16),
            VMEM(shift_weight.shape, BF16), VMEM(scale_weight.shape, BF16), VMEM(gate_weight.shape, BF16),
            VMEM(query_weight.shape, BF16), VMEM(key_weight.shape, BF16), VMEM(value_weight.shape, BF16),
            VMEM((groups, 4 * HEAD, model), BF16),
            VMEM((n_tp,) + wo_shape, BF16),
            VMEM((8, part_width), F32), VMEM((8, part_width), F32),
            VMEM((n_sp, 8, part_width), F32), VMEM((n_tp, 8, part_width), F32),
            VMEM((8, model), F32), VMEM((4, 8, model), F32),
            VMEM((TILE, model), BF16),
            VMEM((n_tiles, HEAD, TILE), F32), VMEM((n_tiles, HEAD, TILE), F32),
            VMEM((n_tiles, groups, 2, HEAD, TILE), BF16),
            VMEM((n_tiles, groups, 128, 128), BF16),
            VMEM((n_tiles, groups, HEAD, TILE), BF16),
            VMEM((groups, HEAD, 128), BF16),
            VMEM((groups, n_tiles, 2, HEAD, TILE), BF16),
            VMEM((n_sp * n_tiles, 128, 128), BF16),
            VMEM((n_sp * n_tiles, HEAD + ONES, TILE), BF16),
            VMEM((n_sp, HEAD, 128), BF16),
            VMEM((n_context, 128, 128), BF16),
            VMEM((n_context, HEAD + ONES, TILE), BF16),
            VMEM((n_q, 128, 2 * TILE), BF16),
            VMEM((most, 128, 2 * TILE), F32), VMEM((most, 128, 2 * TILE), F32),
            VMEM((n_q, 8, TILE), F32), VMEM((n_q, HEAD + ONES, TILE), F32),
            VMEM((n_tiles, groups, per_tile, 2 * HEAD, rows), BF16),
            VMEM((n_tp, groups, 2 * HEAD, rows), BF16),
            VMEM((rows, n_tp * groups * 2 * HEAD), BF16),
            dma((9,)), dma((n_sp,)), dma((n_sp,)), dma((n_tp,)), dma((n_tp,)),
            dma((n_y, l_chunks)), dma((n_tp, l_chunks)), dma((1 + n_y, l_chunks)), dma((n_tp, l_chunks)),
            dma((n_tiles, groups)), dma((groups, n_tiles)),
            dma((n_tiles, n_sp)), dma((n_sp, n_tiles)), dma((n_tiles, n_sp)), dma((n_sp, n_tiles)),
            dma((n_sp,)), dma((n_sp,)),
            dma((n_y, w_chunks)), dma((n_tp, w_chunks)), dma((n_y, w_chunks)), dma((n_tp, w_chunks)),
            dma((n_y, w_chunks, 2)), dma((n_tp, w_chunks, 2)), dma, dma,
            dma((n_tiles, groups, per_tile)), dma((n_tp, groups)),
        ],
        compiler_params=pltpu.CompilerParams(
            collective_id=0, has_side_effects=True, vmem_limit_bytes=60 * 1024 * 1024
        ),
    )(
        latent, context, conditioning[None], context_conditioning[None],
        shift_weight, scale_weight, gate_weight, norm_gain[None],
        query_weight, key_weight, value_weight,
        query_gain[:, None], key_gain[:, None], context_lift, output_weight.reshape(wo_shape),
    )


def solution(mesh):
    n_sp, n_tp = mesh.shape["sp"], mesh.shape["tp"]
    in_specs = (
        P(("sp", "tp"), None), P("sp", None), P("sp"), P("sp"),
        P("sp", "tp"), P("sp", "tp"), P("sp", "tp"), P(),
        P(None, "tp"), P(None, "tp"), P(None, "tp"), P(), P(), P("tp"), P("tp", None),
    )
    body = functools.partial(shards, n_sp, n_tp)
    return jax.shard_map(body, mesh=mesh, in_specs=in_specs, out_specs=P(("sp", "tp"), None), check_vma=False)
```

time: 116 us -> 84.2 us (0.73)
  Pallas kernels: 104 us -> 79.4 us
  matrix products: 5.65 us -> 0 us
  local copies, waits for them, and re-layouts: 5.98 us -> 4.58 us
    pallas_call x2 -> x1, Pallas kernels: 104 us -> 79.4 us  [shards(): pl.pallas_call(functools.partial(fused_kernel, n_sp, n_tp, groups, w_chun...]
    dot_general x1 -> x0, matrix products: 5.65 us -> none  [shards(): jnp.dot(jnp.transpose(by_rows, (1, 0, 2)).reshape(rows, n_tp * o_rows), w...]
    another operation x11 -> x0, local copies, waits for them, and re-layouts: 4.49 us -> none  [the longest x7 1.99 us: rotary_tables(): return (jnp.tile(cos_t, (1, 2)), jnp.tile(sin_t, (1, 2)))]
    broadcast_in_dim x2, local copies, waits for them, and re-layouts: 0.09 us -> 2.7 us  [the longest x1 1.36 us: shards(): query_gain[:, None]]
    unnamed x0 -> x1, local copies, waits for them, and re-layouts: none -> 1.88 us
    transpose x1 -> x0, local copies, waits for them, and re-layouts: 1.31 us -> none  [shards(): jnp.transpose(by_rows, (1, 0, 2)).reshape(rows, n_tp * o_rows)]
where the time goes in v1:
time: 84.2 us; the launch traced here: 84 us
  Pallas kernels  79.4 us (94%)
  local copies, waits for them, and re-layouts  4.58 us (5%)
    pallas_call x1, Pallas kernels, shards(): pl.pallas_call(functools.partial(fused_kernel, n_sp, n_tp, groups, w_chun...  79.4 us
    unnamed x1, local copies, waits for them, and re-layouts  1.88 us

profile of v1, /device:TPU:1, one launch (start us, length us, event | category | flops | bytes accessed | tf_op | source)
XLA Modules:
  0.0 84.0 jit_solution(1119976322712038202)
XLA Ops:
  0.0 1.4 %copy.16.q_gain = f32[64,1]{1,0:T(8,128)} copy(f32[64,1]{0,1:T(1,128)} %bitcast.10) | data formatting | bytes 512 | tf_op jit(solution)/shard_map/broadcast_in_dim | solution.py:710
  1.4 1.3 %copy.17.k_gain = f32[64,1]{1,0:T(8,128)} copy(f32[64,1]{0,1:T(1,128)} %bitcast.11) | data formatting | bytes 512 | tf_op jit(solution)/shard_map/broadcast_in_dim | solution.py:710
  2.7 79.4 %fused.1 = bf16[128,2048]{1,0:T(8,128)(2,1)} custom-call(bf16[128,2048]{1,0:T(8,128)(2,1)} %latent_h.1, bf16[64,2048]{1,0:T(8,128)(2,1)} %context_h.1, f32[1,256]{1,0:T(1,128)} %bitcast.8, f32[1,256]{1,0:T(1,128)} %bitcast.9, bf16[256,512]{1,0:T(8,128)(2,1)} %shift_h.1, bf16[256,512]{1,0:T(8,128)(2,1)} %scale_h.1, bf16[256,512]{1,0:T(8,128)(2,1)} %gate_h.1, ...), custom_call_target="tpu_custom_call" | custom-call | tf_op jit(solution)/shard_map/fused/pallas_call | solution.py:659
  82.1 1.9 %copy.19 = bf16[128,2048]{1,0:T(8,128)(2,1)} copy(bf16[128,2048]{1,0:T(8,128)(2,1)} %fused.1) | data formatting | bytes 1048576

commit v2 on v1

--- a/solution.py
+++ b/solution.py
@@ -47,8 +47,16 @@
     lax.fori_loop(low, high, step, 0)
 
 
+def few(low, high, body):
+    if high - low > 16:
+        loop(low, high, body)
+    else:
+        for i in range(low, high):
+            body(i)
+
+
 def fused_kernel(
-    n_sp, n_tp, groups, w_chunks, l_chunks,
+    n_sp, n_tp, groups, n_x, n_z, plain, l_chunks,
     latent_h, context_h, cond, ctx_cond, shift_h, scale_h, gate_h, gain,
     wq_h, wk_h, wv_h, q_gain, k_gain, lift, wo_h,
     out,
@@ -95,12 +103,12 @@
     def greet(sp, tp):
         pl.semaphore_signal(barrier, inc=1, device_id=(sp, tp), device_id_type=pl.DeviceIdType.MESH)
 
-    loop(1, n_sp, lambda j: greet(lax.rem(me + j, n_sp), t))
-
-    def greet_half(j):
-        loop(1, n_tp, lambda i: greet(half * groups + j, lax.rem(t + i, n_tp)))
-
-    loop(0, groups, greet_half)
+    def greet_half(i):
+        to = lax.rem(t + 1 + i // groups, n_tp)
+        greet(half * groups + lax.rem(g + i, groups), to)
+
+    few(1, n_sp, lambda j: greet(lax.rem(me + j, n_sp), t))
+    few(0, groups * (n_tp - 1), greet_half)
     pl.semaphore_wait(barrier, n_sp - 1 + groups * (n_tp - 1))
 
     piece = rows // l_chunks
@@ -114,7 +122,8 @@
     def y_start(ch):
         loop(1, n_y, lambda k: y_copy(k, ch).start())
 
-    early = (l_chunks + 1) // 2
+    early = (l_chunks + 1) * 2 // 5
+    early = max(early, 1)
     for ch in range(early):
         y_start(ch)
     own_partner = remote(lat.at[t], lat.at[t], sfw.at[0, 0], rp.at[t, 0], me, partner)
@@ -218,8 +227,11 @@
         x = (x * inv).reshape(x.shape[0] // 8, 8, model)
         return (x * rows8[2 * which][None] + rows8[2 * which + 1][None]).reshape(-1, model)
 
-    q_gains = jnp.broadcast_to(q_gain[...], (HEAD, TILE))
-    k_gains = jnp.broadcast_to(k_gain[...], (HEAD, TILE))
+    def column(row):
+        turned = jnp.transpose(jnp.broadcast_to(row[...], (128, HEAD)))
+        return jnp.concatenate([turned] * (TILE // 128), axis=1)
+
+    q_gains, k_gains = column(q_gain), column(k_gain)
 
     def norm(v, gains):
         mean = jnp.mean(v * v, axis=0, keepdims=True)
@@ -245,13 +257,19 @@
             ),
         )
 
+    def hide(owner):
+        base = lax.rem(owner, per_tile) * rows
+
+        def one(i):
+            x = lat[owner, pl.ds(i * step_rows, step_rows), :]
+            start = pl.multiple_of(base + i * step_rows, step_rows)
+            hid[pl.ds(start, step_rows), :] = hidden_of(x, 0).astype(BF16)
+
+        loop(0, rows // step_rows, one)
+
+    border = (half == 0) == (g >= groups // 2) if halves == 2 else g >= 0
+
     def project(bk):
-        def hide(i):
-            start = i * step_rows
-            x = lat[bk * per_tile + start // rows, pl.ds(start % rows, step_rows), :]
-            hid[pl.ds(pl.multiple_of(start, step_rows), step_rows), :] = hidden_of(x, 0).astype(BF16)
-
-        loop(0, TILE // step_rows, hide)
         cos_v, sin_v = cos_t[bk], sin_t[bk]
         order = [lax.rem(g + n, groups) for n in list(range(1, groups)) + [0]]
         ahead = dot_nt(w_t[order[0]], hid[...])
@@ -271,15 +289,23 @@
                 q_copy(bk, j, n).start()
                 for copy in kv_copies(bk, n):
                     copy.start()
+
+            @pl.when(border)
+            def _(n=n):
+                for d in range(1, halves):
+                    for copy in kv_copies(bk, d * groups + n):
+                        copy.start()
+
         qin[g, bk] = qst[bk, g]
         kin[me * n_tiles + bk] = kst[bk, g]
         vin[me * n_tiles + bk, 0:HEAD, :] = vst[bk, g]
 
-        def cross(n):
+    def cross(bk):
+        def one(n):
             for copy in kv_copies(bk, n):
                 copy.start()
 
-        loop(groups, n_sp, cross)
+        loop(groups, n_sp, one)
 
     def y_near(other):
         return other * 2 + c, other * 2 + 1 - c
@@ -295,15 +321,18 @@
             part_of = lat.at[near, pl.ds(ch * piece, piece)]
             pltpu.make_async_copy(part_of, part_of, ry.at[near, ch]).wait()
             forward(other, ch).start()
+        hide(near)
         for ch in range(l_chunks):
             part_of = lat.at[far, pl.ds(ch * piece, piece)]
             pltpu.make_async_copy(part_of, part_of, rp.at[far, ch]).wait()
-
+        hide(far)
+
+    hide(t)
     pltpu.make_async_copy(lat.at[partner], lat.at[partner], rp.at[partner, 0]).wait()
+    hide(partner)
     if y_per > 1:
         loop(1, y_per, lambda o: take(own_block * y_per + lax.rem(y % y_per + o, y_per)))
     project(block(0))
-
     fetch[7].wait()
     c_lane = lax.broadcasted_iota(jnp.int32, (HEAD, 128), 1)
 
@@ -328,66 +357,89 @@
     cin[me] = cst[g]
 
     fetch[8].wait()
-    side = me % 2
-    across = me + 1 - 2 * side
+    shared = n_x + n_z
+    side_x, side_z = me % 2, g // (groups // 2 if groups > 1 else 1) % 2
+    across_x = me + 1 - 2 * side_x
+    across_z = half * groups + lax.rem(g + groups // 2, groups)
+
+    def w_ref(owner, at):
+        return wo_all.at[owner, at]
+
+    def w_at(ch, mine=True):
+        if ch < n_x:
+            return (side_x if mine else 1 - side_x) * n_x + ch
+        if ch < shared:
+            return 2 * n_x + (side_z if mine else 1 - side_z) * n_z + ch - n_x
+        return shared + ch
 
     def w_y(k, ch):
         other = lax.rem(y + k, n_y)
-        ref = wo_all.at[t, side, ch]
+        ref = w_ref(t, w_at(ch))
         return remote(ref, ref, swy.at[k, ch], rwy.at[t, ch], me, other * 2 + c)
 
     def w_x(other, ch):
         near, _ = y_near(other)
-        ref = wo_all.at[near, side, ch]
-        return remote(ref, ref, swx.at[other, ch], rwx.at[near, ch], across, t)
-
-    def w_p(other, ch, second):
+        ref = w_ref(near, w_at(ch))
+        return remote(ref, ref, swx.at[other, ch], rwx.at[near, ch], across_x if ch < n_x else across_z, t)
+
+    def w_p(other, ch, mine=True):
         near, _ = y_near(other)
-        ref = wo_all.at[near, 1 - side if second else side, ch]
-        return remote(ref, ref, swp.at[other, ch, second], rwp.at[near, ch, second], me, partner)
+        at = w_at(ch, mine)
+        ref = w_ref(near, at)
+        return remote(ref, ref, swp.at[other, at], rwp.at[near, at], me, partner)
 
     w_own = remote(wo_all.at[t], wo_all.at[t], swo, rwo, me, partner)
 
-    def forward_y(ch):
-        def one(k):
-            other = lax.rem(y + n_y - k, n_y)
+    def over_y(body):
+        loop(1, n_y, lambda k: body(lax.rem(y + n_y - k, n_y)))
+
+    def forward_y(ch, to_x=True):
+        def one(other):
             near, _ = y_near(other)
-            ref = wo_all.at[near, side, ch]
+            ref = w_ref(near, w_at(ch))
             pltpu.make_async_copy(ref, ref, rwy.at[near, ch]).wait()
-            w_x(other, ch).start()
-            w_p(other, ch, 0).start()
-
-        loop(1, n_y, one)
+            if to_x:
+                w_x(other, ch).start()
+            w_p(other, ch).start()
+
+        over_y(one)
 
     def forward_x(ch):
-        def one(k):
-            other = lax.rem(y + n_y - k, n_y)
+        def one(other):
             near, _ = y_near(other)
-            ref = wo_all.at[near, 1 - side, ch]
+            ref = w_ref(near, w_at(ch, False))
             pltpu.make_async_copy(ref, ref, rwx.at[near, ch]).wait()
-            w_p(other, ch, 1).start()
-
-        loop(1, n_y, one)
-
-    for ch in range(w_chunks):
+            w_p(other, ch, False).start()
+
+        over_y(one)
+
+    def forward_plain(ch):
+        forward_y(shared + ch, False)
+
+    for ch in range(shared + plain):
         loop(1, n_y, lambda k, ch=ch: w_y(k, ch).start())
-    w_own.start()
 
     for k in range(1, n_tiles):
         loop(0, y_per, lambda o, k=k: take(block(k) * y_per + o))
         project(block(k))
-
-    def wait_kv(d, k, low):
+    w_own.start()
+
+    @pl.when(jnp.logical_not(border))
+    def _():
+        for k in range(n_tiles):
+            cross(block(k))
+
+    def wait_kv(d, k, low, high, first):
         bk = block(k)
 
         def one(i):
-            s = lax.rem(half + d, halves) * groups + lax.rem(g + i, groups)
+            s = lax.rem(half + d, halves) * groups + lax.rem(first + i, groups)
             slot = s * n_tiles + bk
             pltpu.make_async_copy(kin.at[slot], kin.at[slot], rk.at[s, bk]).wait()
             ref = vin.at[slot, pl.ds(0, HEAD)]
             pltpu.make_async_copy(ref, ref, rv.at[s, bk]).wait()
 
-        loop(low, groups, one)
+        loop(low, high, one)
 
     def wait_own(k):
         bk = block(k)
@@ -397,7 +449,7 @@
             pltpu.make_async_copy(qin.at[j, bk], qin.at[j, bk], rq.at[j, bk]).wait()
 
         loop(1, groups, one)
-        wait_kv(0, k, 1)
+        wait_kv(0, k, 1, groups, g)
 
         def spread(j):
             for i in range(2):
@@ -409,7 +461,7 @@
         loop(0, groups, spread)
 
     def wait_cross(d, k):
-        wait_kv(d, k, 0)
+        wait_kv(d, k, 0, groups, 0)
 
     def wait_context():
         def one(j):
@@ -434,9 +486,9 @@
             kcx[u] = jnp.transpose(jnp.concatenate(keys, axis=0)).astype(BF16)
             vcx[u, 0:HEAD, :] = jnp.concatenate(values, axis=1).astype(BF16)
 
-    def slabs(d, k):
+    def slabs(d, k, first=0, count=groups):
         base = lax.rem(half + d, halves) * groups
-        slots = [(base + i) * n_tiles + block(k) for i in range(groups)]
+        slots = [(base + first + i) * n_tiles + block(k) for i in range(count)]
         return [(kin, vin, slot, False) for slot in slots]
 
     context = [(kcx, vcx, u, True) for u in range(kcx.shape[0])]
@@ -447,7 +499,14 @@
             half * groups + j, bk * per_tile + p,
         )
 
-    def sweep(k, blocks, start, final):
+    def hooks(actions):
+        def at(j):
+            for when, action in actions.items():
+                pl.when(j == when)(action)
+
+        return at
+
+    def sweep(k, blocks, start, final, hook=None):
         bk = block(k)
 
         def slot_of(j, i):
@@ -499,6 +558,8 @@
             later = pair(j, top)
             top = scores(j + 1, 0, sa)
             soft(j, 1, sb, later)
+            if hook is not None:
+                hook(j)
             if final:
                 for p in range(per_tile):
                     out_copy(bk, lax.rem(g + 1 + j, groups), p).start()
@@ -521,24 +582,41 @@
             if k == 0:
                 att_t[t, g] = ost[bk, g, t % per_tile]
 
-    if n_tiles == 2 and halves == 2:
+    if n_tiles == 2 and halves == 2 and groups == 4 and shared == 7:
+        near_g = jnp.where(half == 0, 0, groups // 2)
+        far_g = groups // 2 - near_g
+        near, close = slabs(1, 0, near_g, 2), slabs(1, 1, near_g, 2)
+        far0, far1 = slabs(1, 0, far_g, 2), slabs(1, 1, far_g, 2)
         wait_own(0)
+        forward_y(0)
         sweep(0, slabs(0, 0), True, False)
-        wait_cross(1, 0)
+        forward_y(1)
+        wait_kv(1, 0, 0, 2, near_g)
         wait_context()
-        sweep(0, slabs(1, 0) + context, False, False)
+        sweep(0, near + context, False, False)
+        forward_y(2)
         wait_own(1)
-        forward_y(0)
-        sweep(1, slabs(0, 0) + slabs(0, 1) + context + slabs(1, 0), True, False)
-        for ch in range(1, w_chunks - 1):
-            forward_y(ch)
+        own = slabs(0, 0) + slabs(0, 1) + context + near
+        sweep(1, own, True, False, hooks({1: lambda: forward_y(3)}))
+        forward_y(4)
+        forward_y(5)
         forward_x(0)
-        wait_cross(1, 1)
-        sweep(1, slabs(1, 1), False, True)
-        forward_y(w_chunks - 1)
-        sweep(0, slabs(0, 1) + slabs(1, 1), False, True)
-        for ch in range(1, w_chunks):
-            forward_x(ch)
+        sweep(0, slabs(0, 1), False, False)
+        forward_y(6)
+        forward_x(1)
+        wait_kv(1, 1, 0, 2, near_g)
+        wait_kv(1, 0, 0, 2, far_g)
+        wait_kv(1, 1, 0, 2, far_g)
+        far = close + far0 + far1
+        forward_plain(0)
+        forward_x(2)
+        sweep(1, far, False, True)
+        forward_plain(1)
+        forward_x(3)
+        sweep(0, far, False, True)
+        forward_x(4)
+        forward_x(5)
+        forward_x(6)
     else:
         for k in range(n_tiles):
             wait_own(k)
@@ -556,9 +634,11 @@
         if halves > 1:
             loop(1, halves - 1, lambda d: further(d, False))
             further(halves - 1, True)
-        for ch in range(w_chunks):
+        for ch in range(shared):
             forward_y(ch)
-        for ch in range(w_chunks):
+        for ch in range(plain):
+            forward_plain(ch)
+        for ch in range(shared):
             forward_x(ch)
 
     ref = wo_all.at[partner]
@@ -566,10 +646,9 @@
 
     def w_far(k):
         _, far = y_near(lax.rem(y + n_y - k, n_y))
-        for ch in range(w_chunks):
-            for second in range(2):
-                ref = wo_all.at[far, 1 - side if second else side, ch]
-                pltpu.make_async_copy(ref, ref, rwp.at[far, ch, second]).wait()
+        for at in range(2 * shared + plain):
+            ref = w_ref(far, at)
+            pltpu.make_async_copy(ref, ref, rwp.at[far, at]).wait()
 
     loop(1, n_y, w_far)
 
@@ -587,7 +666,7 @@
     wide = model // n_out
     for n in range(n_out):
         span = slice(n * wide, (n + 1) * wide)
-        weight = wo_all[:, :, :, :, span].reshape(-1, wide)
+        weight = wo_all[:, :, :, span].reshape(-1, wide)
         projection = dot(att[...], weight)
         out[:, span] = (lat[t, :, span].astype(F32) + mods[4:5, span] * projection).astype(BF16)
 
@@ -599,11 +678,12 @@
         for ch in range(l_chunks):
             y_copy(k, ch).wait_send()
             forward(other, ch).wait_send()
-        for ch in range(w_chunks):
+        for ch in range(shared + plain):
             w_y(k, ch).wait_send()
+            w_p(other, ch).wait_send()
+        for ch in range(shared):
             w_x(other, ch).wait_send()
-            w_p(other, ch, 0).wait_send()
-            w_p(other, ch, 1).wait_send()
+            w_p(other, ch, False).wait_send()
 
     loop(1, n_y, drain_y)
     loop(1, n_sp, lambda j: mod_copy(j).wait_send())
@@ -646,8 +726,10 @@
     per_tile = TILE // rows
     n_tiles = rows * n_tp // TILE
     n_context = n_sp * c_rows // TILE
-    w_chunks = 4 if o_rows >= 256 else 1
-    l_chunks = 4 if rows >= 64 else 1
+    n_x, n_z, plain = (5, 2, 2) if o_rows >= 256 and groups == 4 else (1, 0, 0)
+    shared = n_x + n_z
+    pieces = 2 * shared + plain
+    l_chunks = 8 if rows >= 128 else 1
     most = groups * n_tiles * 2 + n_context
     n_q = groups * n_tiles * 2
     n_y = n_tp // 2
@@ -655,9 +737,9 @@
     dma = pltpu.SemaphoreType.DMA
     hbm = pl.BlockSpec(memory_space=pltpu.HBM)
     smem = pl.BlockSpec(memory_space=pltpu.SMEM)
-    wo_shape = (2, w_chunks, o_rows // (2 * w_chunks), model)
+    wo_shape = (pieces, o_rows // pieces, model)
     return pl.pallas_call(
-        functools.partial(fused_kernel, n_sp, n_tp, groups, w_chunks, l_chunks),
+        functools.partial(fused_kernel, n_sp, n_tp, groups, n_x, n_z, plain, l_chunks),
         name="fused",
         out_shape=jax.ShapeDtypeStruct((rows, model), BF16),
         in_specs=[
@@ -696,8 +778,8 @@
             dma((n_tiles, groups)), dma((groups, n_tiles)),
             dma((n_tiles, n_sp)), dma((n_sp, n_tiles)), dma((n_tiles, n_sp)), dma((n_sp, n_tiles)),
             dma((n_sp,)), dma((n_sp,)),
-            dma((n_y, w_chunks)), dma((n_tp, w_chunks)), dma((n_y, w_chunks)), dma((n_tp, w_chunks)),
-            dma((n_y, w_chunks, 2)), dma((n_tp, w_chunks, 2)), dma, dma,
+            dma((n_y, pieces)), dma((n_tp, pieces)), dma((n_y, shared)), dma((n_tp, shared)),
+            dma((n_y, pieces)), dma((n_tp, pieces)), dma, dma,
             dma((n_tiles, groups, per_tile)), dma((n_tp, groups)),
         ],
         compiler_params=pltpu.CompilerParams(
@@ -707,7 +789,7 @@
         latent, context, conditioning[None], context_conditioning[None],
         shift_weight, scale_weight, gate_weight, norm_gain[None],
         query_weight, key_weight, value_weight,
-        query_gain[:, None], key_gain[:, None], context_lift, output_weight.reshape(wo_shape),
+        query_gain[None], key_gain[None], context_lift, output_weight.reshape(wo_shape),
     )
 
 

time: 84.2 us -> 70 us (0.83)
  Pallas kernels: 79.4 us -> 67.5 us
  local copies, waits for them, and re-layouts: 4.58 us -> 1.88 us
    pallas_call x1, Pallas kernels: 79.4 us -> 67.5 us  [shards(): pl.pallas_call(functools.partial(fused_kernel, n_sp, n_tp, groups, n_x, n...]
    broadcast_in_dim x2 -> x0, local copies, waits for them, and re-layouts: 2.7 us -> none  [the longest x1 1.36 us: shards(): query_gain[:, None]]
where the time goes in v2:
time: 70 us; the launch traced here: 69.3 us
  Pallas kernels  67.5 us (96%)
  local copies, waits for them, and re-layouts  1.88 us (3%)
    pallas_call x1, Pallas kernels, shards(): pl.pallas_call(functools.partial(fused_kernel, n_sp, n_tp, groups, n_x, n...  67.5 us
    unnamed x1, local copies, waits for them, and re-layouts  1.88 us

profile of v2, /device:TPU:1, one launch (start us, length us, event | category | flops | bytes accessed | tf_op | source)
XLA Modules:
  0.0 69.3 jit_solution(5902962415667004020)
XLA Ops:
  0.0 67.5 %fused.1 = bf16[128,2048]{1,0:T(8,128)(2,1)} custom-call(bf16[128,2048]{1,0:T(8,128)(2,1)} %latent_h.1, bf16[64,2048]{1,0:T(8,128)(2,1)} %context_h.1, f32[1,256]{1,0:T(1,128)} %bitcast.8, f32[1,256]{1,0:T(1,128)} %bitcast.9, bf16[256,512]{1,0:T(8,128)(2,1)} %shift_h.1, bf16[256,512]{1,0:T(8,128)(2,1)} %scale_h.1, bf16[256,512]{1,0:T(8,128)(2,1)} %gate_h.1, ...), custom_call_target="tpu_custom_call" | custom-call | tf_op jit(solution)/shard_map/fused/pallas_call | solution.py:741
  67.5 1.9 %copy.17 = bf16[128,2048]{1,0:T(8,128)(2,1)} copy(bf16[128,2048]{1,0:T(8,128)(2,1)} %fused.1) | data formatting | bytes 1048576

commit v3 on v2

--- a/solution.py
+++ b/solution.py
@@ -86,6 +86,17 @@
     def block(k):
         return lax.rem(own_block + k, n_tiles)
 
+    barrier = pltpu.get_barrier_semaphore()
+
+    def greet(sp, tp):
+        pl.semaphore_signal(barrier, inc=1, device_id=(sp, tp), device_id_type=pl.DeviceIdType.MESH)
+
+    def greet_half(i):
+        to = lax.rem(t + 1 + i // groups, n_tp)
+        greet(half * groups + lax.rem(g + i, groups), to)
+
+    few(1, n_sp, lambda j: greet(lax.rem(me + j, n_sp), t))
+    few(0, groups * (n_tp - 1), greet_half)
     fetch = [
         pltpu.make_async_copy(src, dst, loads.at[i])
         for i, (src, dst) in enumerate(
@@ -98,17 +109,6 @@
     ]
     for copy in fetch:
         copy.start()
-    barrier = pltpu.get_barrier_semaphore()
-
-    def greet(sp, tp):
-        pl.semaphore_signal(barrier, inc=1, device_id=(sp, tp), device_id_type=pl.DeviceIdType.MESH)
-
-    def greet_half(i):
-        to = lax.rem(t + 1 + i // groups, n_tp)
-        greet(half * groups + lax.rem(g + i, groups), to)
-
-    few(1, n_sp, lambda j: greet(lax.rem(me + j, n_sp), t))
-    few(0, groups * (n_tp - 1), greet_half)
     pl.semaphore_wait(barrier, n_sp - 1 + groups * (n_tp - 1))
 
     piece = rows // l_chunks
@@ -441,7 +441,7 @@
 
         loop(low, high, one)
 
-    def wait_own(k):
+    def wait_queries(k):
         bk = block(k)
 
         def one(i):
@@ -449,7 +449,6 @@
             pltpu.make_async_copy(qin.at[j, bk], qin.at[j, bk], rq.at[j, bk]).wait()
 
         loop(1, groups, one)
-        wait_kv(0, k, 1, groups, g)
 
         def spread(j):
             for i in range(2):
@@ -459,6 +458,10 @@
                 qbd[slot, HEAD:, TILE:] = q
 
         loop(0, groups, spread)
+
+    def wait_own(k):
+        wait_queries(k)
+        wait_kv(0, k, 1, groups, g)
 
     def wait_cross(d, k):
         wait_kv(d, k, 0, groups, 0)
@@ -499,14 +502,7 @@
             half * groups + j, bk * per_tile + p,
         )
 
-    def hooks(actions):
-        def at(j):
-            for when, action in actions.items():
-                pl.when(j == when)(action)
-
-        return at
-
-    def sweep(k, blocks, start, final, hook=None):
+    def sweep(k, blocks, start, final):
         bk = block(k)
 
         def slot_of(j, i):
@@ -558,8 +554,6 @@
             later = pair(j, top)
             top = scores(j + 1, 0, sa)
             soft(j, 1, sb, later)
-            if hook is not None:
-                hook(j)
             if final:
                 for p in range(per_tile):
                     out_copy(bk, lax.rem(g + 1 + j, groups), p).start()
@@ -582,7 +576,7 @@
             if k == 0:
                 att_t[t, g] = ost[bk, g, t % per_tile]
 
-    if n_tiles == 2 and halves == 2 and groups == 4 and shared == 7:
+    if n_tiles == 2 and halves == 2 and groups == 4 and shared == 6:
         near_g = jnp.where(half == 0, 0, groups // 2)
         far_g = groups // 2 - near_g
         near, close = slabs(1, 0, near_g, 2), slabs(1, 1, near_g, 2)
@@ -593,30 +587,31 @@
         forward_y(1)
         wait_kv(1, 0, 0, 2, near_g)
         wait_context()
+        forward_y(2)
         sweep(0, near + context, False, False)
-        forward_y(2)
-        wait_own(1)
-        own = slabs(0, 0) + slabs(0, 1) + context + near
-        sweep(1, own, True, False, hooks({1: lambda: forward_y(3)}))
+        wait_queries(1)
+        forward_y(3)
+        sweep(1, slabs(0, 0) + context + near, True, False)
         forward_y(4)
         forward_y(5)
+        wait_kv(0, 1, 1, groups, g)
         forward_x(0)
+        forward_x(1)
         sweep(0, slabs(0, 1), False, False)
-        forward_y(6)
-        forward_x(1)
         wait_kv(1, 1, 0, 2, near_g)
         wait_kv(1, 0, 0, 2, far_g)
         wait_kv(1, 1, 0, 2, far_g)
         far = close + far0 + far1
         forward_plain(0)
+        sweep(1, slabs(0, 1) + far, False, True)
+        forward_plain(1)
+        forward_plain(2)
         forward_x(2)
-        sweep(1, far, False, True)
-        forward_plain(1)
         forward_x(3)
         sweep(0, far, False, True)
+        forward_plain(3)
         forward_x(4)
         forward_x(5)
-        forward_x(6)
     else:
         for k in range(n_tiles):
             wait_own(k)
@@ -726,7 +721,7 @@
     per_tile = TILE // rows
     n_tiles = rows * n_tp // TILE
     n_context = n_sp * c_rows // TILE
-    n_x, n_z, plain = (5, 2, 2) if o_rows >= 256 and groups == 4 else (1, 0, 0)
+    n_x, n_z, plain = (4, 2, 4) if o_rows >= 256 and groups == 4 else (1, 0, 0)
     shared = n_x + n_z
     pieces = 2 * shared + plain
     l_chunks = 8 if rows >= 128 else 1

time: 70 us -> 68.9 us (0.984)
  Pallas kernels: 67.5 us -> 66.4 us
    pallas_call x1, Pallas kernels: 67.5 us -> 66.4 us  [shards(): pl.pallas_call(functools.partial(fused_kernel, n_sp, n_tp, groups, n_x, n...]
where the time goes in v3:
time: 68.9 us; the launch traced here: 68.3 us
  Pallas kernels  66.4 us (96%)
  local copies, waits for them, and re-layouts  1.88 us (3%)
    pallas_call x1, Pallas kernels, shards(): pl.pallas_call(functools.partial(fused_kernel, n_sp, n_tp, groups, n_x, n...  66.4 us
    unnamed x1, local copies, waits for them, and re-layouts  1.88 us

profile of v3, /device:TPU:1, one launch (start us, length us, event | category | flops | bytes accessed | tf_op | source)
XLA Modules:
  0.0 68.3 jit_solution(5704704401190865687)
XLA Ops:
  0.0 66.4 %fused.1 = bf16[128,2048]{1,0:T(8,128)(2,1)} custom-call(bf16[128,2048]{1,0:T(8,128)(2,1)} %latent_h.1, bf16[64,2048]{1,0:T(8,128)(2,1)} %context_h.1, f32[1,256]{1,0:T(1,128)} %bitcast.8, f32[1,256]{1,0:T(1,128)} %bitcast.9, bf16[256,512]{1,0:T(8,128)(2,1)} %shift_h.1, bf16[256,512]{1,0:T(8,128)(2,1)} %scale_h.1, bf16[256,512]{1,0:T(8,128)(2,1)} %gate_h.1, ...), custom_call_target="tpu_custom_call" | custom-call | tf_op jit(solution)/shard_map/fused/pallas_call | solution.py:736
  66.4 1.9 %copy.17 = bf16[128,2048]{1,0:T(8,128)(2,1)} copy(bf16[128,2048]{1,0:T(8,128)(2,1)} %fused.1) | data formatting | bytes 1048576
